TPU v7x, 32 devices: a whole 2x2x4 slice. The times are simulated.
32 devices in a mesh: ep: 8 (over z, y), tp: 4 (over x, core).
Axes of the slice: x: 2, y: 2, z: 4, core: 2. Of those that a mesh axis runs over, the one named last changes fastest.
Arguments:
- queries_a: bfloat16 [1024, 1024], P('ep', 'tp'), may hold values from -128 to 128
- queries_b: bfloat16 [1024, 1024], P('ep', 'tp'), may hold values from -128 to 128
- keys_a: bfloat16 [1024, 512], P('ep', 'tp'), may hold values from -8 to 8
- keys_b: bfloat16 [1024, 512], P('ep', 'tp'), may hold values from -8 to 8
- values: bfloat16 [1024, 1024], P('ep', 'tp'), may hold values from -6 to 6
- lambdas: float32 [16], P('tp'), may hold values from 0.3 to 0.8
- head_gain: float32 [128], replicated, may hold values from 0.1 to 1.9
- w_out: bfloat16 [2048, 2048], P('tp'), may hold values from -0.125 to 0.125
- moe_tokens: bfloat16 [4096, 2048], P(('ep', 'tp')), may hold values from -80 to 80
- moe_gain: float32 [2048], replicated, may hold values from 0.1 to 1.9
- routes: int32 [4096, 2], P(('ep', 'tp')), may hold values from 0 to 7, all different within a row; in each aligned block of 128 rows (0 to 127, 128 to 255, ...) at most 48 rows name the same one
- route_weights: float32 [4096, 2], P(('ep', 'tp')), may hold values from 0.1 to 1
- w_gate: bfloat16 [8, 2048, 2048], P('ep', None, 'tp'), may hold values from -4 to 4
- w_up: bfloat16 [8, 2048, 2048], P('ep', None, 'tp'), may hold values from -4 to 4
- w_down: bfloat16 [8, 2048, 2048], P('ep', 'tp'), may hold values from -0.0625 to 0.0625
Outputs:
- mixer_out: bfloat16 [1024, 2048], P(('ep', 'tp'))
- moe_out: bfloat16 [4096, 2048], P(('ep', 'tp'))
Inputs may be any that keep to these rules, and one draw needn't show every extreme that they name: `routes`: each row names 2 different experts. Within the rows of one device no expert is named by more than 48 rows, a bound that some block reaches of some device.
All inputs are finite; a program needn't handle non-finite values.
Results may differ from a plain program's by a relative error of at most 0.011.
Values may be sent and summed in bfloat16 or wider, within the bound.
A program may use at most 192 MiB of HBM per device.

v0:
```python
import jax
import jax.numpy as jnp
from jax import lax
from jax.sharding import PartitionSpec as P

HEAD = 64
VDIM = 128
TOP = 2
eps = 1e-05
alpha_act = 1.702
limit_act = 7.0
negative = -1e30


def clamped_unit(gate, up):
    capped = jnp.minimum(gate, limit_act)
    linear = jnp.clip(up, -limit_act, limit_act)
    return capped * jax.nn.sigmoid(alpha_act * capped) * (linear + 1.0)


def hidden_rows(inputs, gate_matrix, up_matrix):
    gate = jnp.dot(inputs, gate_matrix, preferred_element_type=jnp.float32)
    up = jnp.dot(inputs, up_matrix, preferred_element_type=jnp.float32)
    return clamped_unit(gate, up).astype(jnp.bfloat16)


def pick_rows(table, owner):
    valid = owner < table.shape[0]
    chosen = jnp.take(table, jnp.minimum(owner, table.shape[0] - 1), axis=0)
    return jnp.where(valid[:, None], chosen, jnp.zeros_like(chosen))


def mixer(queries_a, queries_b, keys_a, keys_b, values, lambdas, head_gain, w_out):
    tokens = queries_a.shape[0]
    local_heads = lambdas.shape[0]
    kv_local = keys_a.shape[1] // HEAD
    group = local_heads // kv_local
    scale = HEAD ** (-0.5)
    query_pos = lax.axis_index("ep") * tokens + jnp.arange(tokens, dtype=jnp.int32)
    grouped_a = queries_a.reshape(tokens, kv_local, group, HEAD)
    grouped_b = queries_b.reshape(tokens, kv_local, group, HEAD)
    lowest = jnp.full((kv_local, group, tokens), negative, jnp.float32)
    nothing = jnp.zeros((kv_local, group, tokens), jnp.float32)
    blank = jnp.zeros((kv_local, group, tokens, VDIM), jnp.float32)

    def one_map(grouped, keys, value_rows, visible, state):
        peak, total, accum = state
        scores = (
            jnp.einsum("rgjd,ngd->gjrn", grouped, keys, preferred_element_type=jnp.float32) * scale
        )
        scores = jnp.where(visible, scores, negative)
        new_peak = jnp.maximum(peak, jnp.max(scores, axis=-1))
        expo = jnp.where(visible, jnp.exp(scores - new_peak[..., None]), 0.0)
        total = jnp.sum(expo, axis=-1)
        accum = jnp.einsum(
            "gjrn,ngv->gjrv",
            expo.astype(jnp.bfloat16),
            value_rows,
            preferred_element_type=jnp.float32,
        )
        return (new_peak, total, accum)

    initial = (lowest, nothing, blank, lowest, nothing, blank)
    piece_a = lax.all_gather(keys_a, "ep", axis=0, tiled=True)
    piece_b = lax.all_gather(keys_b, "ep", axis=0, tiled=True)
    piece_v = lax.all_gather(values, "ep", axis=0, tiled=True)
    count = piece_a.shape[0]

    def visit(state):
        key_pos = jnp.arange(count, dtype=jnp.int32)
        visible = key_pos[None, :] <= query_pos[:, None]
        value_rows = piece_v.reshape(count, kv_local, VDIM)
        first = one_map(
            grouped_a, piece_a.reshape(count, kv_local, HEAD), value_rows, visible, state[:3]
        )
        second = one_map(
            grouped_b, piece_b.reshape(count, kv_local, HEAD), value_rows, visible, state[3:]
        )
        return first + second

    result = lax.cond(jnp.int32(0) <= query_pos[tokens - 1], visit, lambda state: state, initial)
    mixed_a = result[2] / result[1][..., None]
    mixed_b = result[5] / result[4][..., None]
    diff = mixed_a - lambdas.reshape(kv_local, group, 1, 1) * mixed_b
    heads_out = (
        diff * lax.rsqrt(jnp.mean(diff * diff, axis=-1, keepdims=True) + eps) * head_gain
    ).astype(jnp.bfloat16)
    weights_out = w_out.reshape(kv_local, group, VDIM, w_out.shape[1])
    return lax.psum_scatter(
        jnp.einsum(
            "gjrv,gjvd->rd", heads_out, weights_out, preferred_element_type=jnp.float32
        ).astype(jnp.bfloat16),
        "tp",
        scatter_dimension=0,
        tiled=True,
    )


def experts(moe_tokens, moe_gain, routes, route_weights, w_gate, w_up, w_down):
    tok_rows, width = moe_tokens.shape
    n_experts = lax.axis_size("ep") * w_gate.shape[0]
    capacity = max(2, 3 * tok_rows * TOP // (2 * n_experts))
    inputs = moe_tokens.astype(jnp.float32)
    normed = (
        inputs * lax.rsqrt(jnp.mean(inputs * inputs, axis=-1, keepdims=True) + eps) * moe_gain
    ).astype(jnp.bfloat16)
    chosen = routes.reshape(-1)
    member = (chosen[:, None] == jnp.arange(n_experts, dtype=jnp.int32)[None, :]).astype(jnp.int32)
    order_in = jnp.sum(jnp.cumsum(member, axis=0) * member, axis=1) - 1
    slot_ids = chosen * capacity + order_in
    owner = (
        jnp.full((n_experts * capacity,), tok_rows, jnp.int32)
        .at[slot_ids]
        .set(jnp.arange(tok_rows * TOP, dtype=jnp.int32) // TOP)
    )
    outgoing = pick_rows(normed, owner).reshape(n_experts, capacity, width)
    arrived = lax.all_to_all(outgoing, "ep", split_axis=0, concat_axis=1, tiled=True).reshape(
        -1, width
    )
    hidden = hidden_rows(lax.all_gather(arrived, "tp", axis=0, tiled=True), w_gate[0], w_up[0])
    expert_out = lax.psum_scatter(
        jnp.dot(hidden, w_down[0], preferred_element_type=jnp.float32).astype(jnp.bfloat16),
        "tp",
        scatter_dimension=0,
        tiled=True,
    )
    returned = lax.all_to_all(
        expert_out.reshape(-1, capacity, width), "ep", split_axis=0, concat_axis=0, tiled=True
    )
    picked = jnp.take(returned.reshape(-1, width), slot_ids, axis=0).reshape(tok_rows, TOP, width)
    return jnp.sum(picked.astype(jnp.float32) * route_weights[:, :, None], axis=1).astype(
        jnp.bfloat16
    )


def body(
    queries_a,
    queries_b,
    keys_a,
    keys_b,
    values,
    lambdas,
    head_gain,
    w_out,
    moe_tokens,
    moe_gain,
    routes,
    route_weights,
    w_gate,
    w_up,
    w_down,
):
    mixer_out = mixer(queries_a, queries_b, keys_a, keys_b, values, lambdas, head_gain, w_out)
    moe_out = experts(moe_tokens, moe_gain, routes, route_weights, w_gate, w_up, w_down)
    return (mixer_out, moe_out)


def solution(mesh):
    return jax.shard_map(
        body,
        mesh=mesh,
        in_specs=(
            P("ep", "tp"),
            P("ep", "tp"),
            P("ep", "tp"),
            P("ep", "tp"),
            P("ep", "tp"),
            P("tp"),
            P(),
            P("tp", None),
            P(("ep", "tp"), None),
            P(),
            P(("ep", "tp"), None),
            P(("ep", "tp"), None),
            P("ep", None, "tp"),
            P("ep", None, "tp"),
            P("ep", "tp", None),
        ),
        out_specs=(P(("ep", "tp"), None), P(("ep", "tp"), None)),
        check_vma=False,
    )
```

profile of v0, /device:TPU:0, one launch (start us, length us, event | category | flops | bytes accessed | tf_op | source)
XLA Modules:
  0.0 350.4 jit_solution(3916929698931288925)
XLA Ops:
  7.2 0.9 copy.49
  8.2 0.1 eq.26
  8.3 0.1 reshape.159
  8.4 0.7 broadcast_multiply_fusion
  9.1 0.6 reduce-window.6
  9.7 0.2 slice_reduce_fusion
  10.0 0.1 fusion.34
  10.1 0.1 copy.53
  10.2 0.1 mul.117
  10.3 1.4 scatter_custom_fusion
  12.0 1.2 fusion.27
  13.2 1.2 fusion.29
  14.5 3.1 gather_fusion
  17.6 1.7 select_select_fusion
  19.3 44.2 %all_to_all.14 = bf16[8,48,2048]{2,1,0:T(8,128)(2,1)} all-to-all(bf16[8,48,2048]{2,1,0:T(8,128)(2,1)S(1)} %select_select_fusion), channel_id=1, replica_groups=mesh['ep'=8,'tp'=4] {'ep'}, dimensions={0} | all-to-all | bytes 3145728 | tf_op jit(solution)/shard_map/all_to_all | solution.py:117
  63.5 45.5 %all-gather.2.cloned.1.call-done = bf16[1536,2048]{1,0:T(8,128)(2,1)} async-done(((bf16[384,2048]{1,0:T(8,128)(2,1)}), bf16[1536,2048]{1,0:T(8,128)(2,1)}) %all-gather.2.cloned.1.call-update) | async-done | bytes 6291472 | tf_op jit(solution)/shard_map/all_gather | solution.py:120
  109.0 8.5 %convolution_minimum_fusion = f32[1536,512]{1,0:T(8,128)} fusion(bf16[1536,2048]{1,0:T(8,128)(2,1)} %all-gather.2.cloned.1.call-done, bf16[1,2048,512]{2,1,0:T(8,128)(2,1)} %param.29), kind=kOutput, calls=%fused_computation.30 | convolution fusion | flops 3222011904 | bytes 11534336 | tf_op jit(solution)/shard_map/dot_general | solution.py:22
  117.5 11.9 %convolution_convert_fusion = bf16[1536,2048]{1,0:T(8,128)(2,1)} fusion(bf16[1,512,2048]{2,1,0:T(8,128)(2,1)S(1)} %copy-done, bf16[1536,2048]{1,0:T(8,128)(2,1)} %all-gather.2.cloned.1.call-done, f32[1536,512]{1,0:T(8,128)} %convolution_minimum_fusion, bf16[1,2048,512]{2,1,0:T(8,128)(2,1)} %param.30), kind=kOutput, calls=%fused_computation.28 | convolution fusion | flops 6452674560 | bytes 19922944 | tf_op jit(solution)/shard_map/dot_general | solution.py:122
  129.5 58.9 %reduce-scatter.5.cloned.1.call-done = bf16[384,2048]{1,0:T(8,128)(2,1)} async-done(((bf16[1536,2048]{1,0:T(8,128)(2,1)}), bf16[384,2048]{1,0:T(8,128)(2,1)}) %reduce-scatter.5.cloned.1.call-update) | async-done | bytes 1572880 | tf_op jit(solution)/shard_map/reduce_scatter | solution.py:121
  188.4 5.5 %all-to-all-start.1 = ((bf16[8,48,2048]{2,1,0:T(8,128)(2,1)}), bf16[8,48,2048]{2,1,0:T(8,128)(2,1)}, u32[]{:S(2)}, u32[]{:S(2)}) async-start(bf16[8,48,2048]{2,1,0:T(8,128)(2,1)} %bitcast.77), calls=%async_computation.3 | async-start | bytes 3145728 | tf_op jit(solution)/shard_map/all_to_all | solution.py:127
  194.0 0.1 copy.45
  194.1 0.1 copy.46
  194.3 0.6 slice.9
  195.5 0.7 mul.106
  196.2 54.2 %all_gather.12 = bf16[1024,128]{0,1:T(8,128)(2,1)S(1)} all-gather(bf16[128,128]{0,1:T(8,128)(2,1)S(1)} %copy.45), channel_id=1, replica_groups=mesh['ep'=8,'tp'=4] {'ep'}, dimensions={0}, use_global_device_ids=true | all-gather | bytes 294912 | tf_op jit(solution)/shard_map/all_gather | solution.py:64
  250.3 27.8 %all_gather.14 = bf16[1024,128]{0,1:T(8,128)(2,1)} all-gather(bf16[128,128]{0,1:T(8,128)(2,1)S(1)} %copy.46), channel_id=1, replica_groups=mesh['ep'=8,'tp'=4] {'ep'}, dimensions={0}, use_global_device_ids=true | all-gather | bytes 294912 | tf_op jit(solution)/shard_map/all_gather | solution.py:65
  278.2 31.3 %all_gather.13 = bf16[1024,256]{1,0:T(8,128)(2,1)S(1)} all-gather(bf16[128,256]{1,0:T(8,128)(2,1)S(1)} %copy-done.6), channel_id=1, replica_groups=mesh['ep'=8,'tp'=4] {'ep'}, dimensions={0}, use_global_device_ids=true | all-gather | bytes 589824 | tf_op jit(solution)/shard_map/all_gather | solution.py:66
  309.5 12.2 %conditional.1 = (f32[2,2,128]{2,1,0:T(2,128)S(1)}, f32[2,2,128,128]{3,2,1,0:T(8,128)S(1)}, f32[2,2,128]{2,1,0:T(2,128)S(1)}, f32[2,2,128,128]{3,2,1,0:T(8,128)S(1)}) conditional(s32[]{:T(128)} %bitcast.12, () %tuple.16, (s32[128]{0:T(128)S(1)}, bf16[1024,128]{0,1:T(8,128)(2,1)S(1)}, bf16[128,256]{1,0:T(8,128)(2,1)}, bf16[1024,256]{1,0:T(8,128)(2,1)S(1)}, ...), branch_computations={%region_0.0_spmd, %region_1.6_spmd} | conditional | flops 416414720 | bytes 47481572 | solution.py:81
  309.5 0.1 iota_compare_fusion
  309.6 1.0 copy.47
  310.6 1.8 fusion.42
  312.4 0.1 copy.48
  312.5 2.4 fusion.1
  315.0 1.0 fusion.5
  316.0 0.2 copy-done.3
  316.3 0.1 reshape.149
  316.4 0.8 copy-done.5
  317.2 2.6 fusion.6
  319.8 1.9 fusion.8
  321.7 1.0 multiply_reduce_fusion.1
  322.7 2.9 fusion.23
  325.7 0.1 sub.35
  325.9 0.1 copy.52
  326.1 0.1 copy.54
  326.2 4.0 %gather_fusion.1 = bf16[256,2048]{1,0:T(8,128)(2,1)S(1)} fusion(bf16[384,2048]{1,0:T(8,128)(2,1)} %bitcast.26, s32[1024]{0:T(1024)S(1)} %pad_clamp_fusion), kind=kCustom, calls=%fused_computation.1 | custom fusion | bytes 2098176 | tf_op jit(solution)/shard_map/jit(_take)/gather | solution.py:130
  330.2 1.5 gather.15
  331.7 6.2 %multiply_reduce_fusion = bf16[128,2048]{1,0:T(8,128)(2,1)} fusion(bf16[128,2,2048]{2,1,0:T(2,128)(2,1)} %gather.15, pred[128,2]{1,0:T(8,128)(4,1)S(1)} %copy.52, f32[128,2]{1,0:T(8,128)S(1)} %copy.54), kind=kLoop, calls=%fused_computation.39 | loop fusion | flops 1835008 | bytes 1574144 | tf_op jit(solution)/shard_map/reduce_sum | solution.py:131
  338.0 5.9 %reduce-scatter.3.cloned.1.call-done = bf16[32,2048]{1,0:T(8,128)(2,1)} async-done(((bf16[128,2048]{1,0:T(8,128)(2,1)}), bf16[32,2048]{1,0:T(8,128)(2,1)}) %reduce-scatter.3.cloned.1.call-update) | async-done | bytes 131088 | tf_op jit(solution)/shard_map/reduce_scatter | solution.py:89
  (55 shorter events, 0.6 us)
Async XLA Ops:
  7.2 110.4 %copy-start = (bf16[1,512,2048]{2,1,0:T(8,128)(2,1)S(1)}, bf16[1,512,2048]{2,1,0:T(8,128)(2,1)}, u32[]{:S(2)}) copy-start(bf16[1,512,2048]{2,1,0:T(8,128)(2,1)} %param.31) | copy-start | bytes 6291460
  7.2 101.8 %all-gather.2.cloned.1.call-start = ((), (), s32[]{:S(2)}) async-start(), calls=%async_computation.5 | async-start | bytes 7864320 | tf_op jit(solution)/shard_map/all_gather | solution.py:120
  10.3 1.4 copy-start.12
  63.5 124.9 %reduce-scatter.5.cloned.1.call-start = ((), (), s32[]{:S(2)}) async-start(), calls=%async_computation.6 | async-start | bytes 7864320 | tf_op jit(solution)/shard_map/reduce_scatter | solution.py:121
  129.4 64.6 %copy-start.8 = (bf16[128,128]{1,0:T(8,128)(2,1)S(1)}, bf16[128,128]{1,0:T(8,128)(2,1)}, u32[]{:S(2)}) copy-start(bf16[128,128]{1,0:T(8,128)(2,1)} %param.19) | copy-start | bytes 98308
  129.4 64.7 %copy-start.9 = (bf16[128,128]{1,0:T(8,128)(2,1)S(1)}, bf16[128,128]{1,0:T(8,128)(2,1)}, u32[]{:S(2)}) copy-start(bf16[128,128]{1,0:T(8,128)(2,1)} %param.20) | copy-start | bytes 98308
  129.5 66.0 %copy-start.15 = (f32[4]{0:T(128)S(1)}, f32[4]{0:T(128)}, u32[]{:S(2)}) copy-start(f32[4]{0:T(128)} %param.22) | copy-start | bytes 52
  129.5 148.7 %copy-start.6 = (bf16[128,256]{1,0:T(8,128)(2,1)S(1)}, bf16[128,256]{1,0:T(8,128)(2,1)}, u32[]{:S(2)}) copy-start(bf16[128,256]{1,0:T(8,128)(2,1)} %param.21) | copy-start | bytes 196612
  188.4 137.8 %all-to-all-start.1 = ((bf16[8,48,2048]{2,1,0:T(8,128)(2,1)}), bf16[8,48,2048]{2,1,0:T(8,128)(2,1)}, u32[]{:S(2)}, u32[]{:S(2)}) async-start(bf16[8,48,2048]{2,1,0:T(8,128)(2,1)} %bitcast.77), calls=%async_computation.3 | async-start | bytes 3145728 | tf_op jit(solution)/shard_map/all_to_all | solution.py:127
  193.9 149.9 %reduce-scatter.3.cloned.1.call-start = ((), (), s32[]{:S(2)}) async-start(), calls=%async_computation.4 | async-start | bytes 655360 | tf_op jit(solution)/shard_map/reduce_scatter | solution.py:89
  309.5 2.9 copy-start.7
  309.5 3.0 copy-start.4
  312.5 2.5 copy-start.1
  315.0 1.3 copy-start.3
  315.0 1.3 copy-start.11
  316.4 0.8 copy-start.5
  317.2 2.6 copy-start.2
  321.7 4.2 %copy-start.10 = (s32[128,2]{0,1:T(2,128)S(1)}, s32[128,2]{0,1:T(2,128)}, u32[]{:S(2)}) copy-start(s32[128,2]{0,1:T(2,128)} %param.27) | copy-start | bytes 3076
  321.7 4.4 %copy-start.14 = (f32[128,2]{0,1:T(2,128)S(1)}, f32[128,2]{0,1:T(2,128)}, u32[]{:S(2)}) copy-start(f32[128,2]{0,1:T(2,128)} %param.28) | copy-start | bytes 3076
  321.7 4.5 %copy-start.13 = (s32[256,1]{0,1:T(1,128)S(1)}, s32[256,1]{0,1:T(1,128)}, u32[]{:S(2)}) copy-start(s32[256,1]{0,1:T(1,128)} %copy-done.12) | copy-start | bytes 3076
Sparse Core Ops, SparseCore 0:
  63.6 45.3 all-gather.1
  129.6 58.8 reduce-scatter.4
  325.8 18.0 reduce-scatter.2
where the time goes:
time: 351 us; the launch traced here: 350 us
  blocking collectives  158 us (45%)
  waiting for transfers between devices  110 us (31%)
  matrix products  32.1 us (9%)
  local copies, waits for them, and re-layouts  16.1 us (5%)
  between operations  14.7 us (4%)
  other arithmetic  14 us (4%)
  starting transfers between devices  5.63 us (2%)
    reduce_scatter x1, waiting for transfers between devices, experts(): lax.psum_scatter(jnp.dot(hidden, w_down[0], preferred_element_type=jnp.fl...  58.9 us
    all_gather x1, blocking collectives, mixer(): piece_a = lax.all_gather(keys_a, 'ep', axis=0, tiled=True)  54.2 us
    all_gather x1, waiting for transfers between devices, experts(): lax.all_gather(arrived, 'tp', axis=0, tiled=True)  45.5 us
    all_to_all x1, blocking collectives, experts(): lax.all_to_all(outgoing, 'ep', split_axis=0, concat_axis=1, tiled=True)  44.2 us
    all_gather x1, blocking collectives, mixer(): piece_v = lax.all_gather(values, 'ep', axis=0, tiled=True)  31.3 us
    all_gather x1, blocking collectives, mixer(): piece_b = lax.all_gather(keys_b, 'ep', axis=0, tiled=True)  27.8 us
    dot_general x1, matrix products, experts(): jnp.dot(hidden, w_down[0], preferred_element_type=jnp.float32)  11.9 us
    dot_general x1, matrix products, hidden_rows(): gate = jnp.dot(inputs, gate_matrix, preferred_element_type=jnp.float32)  8.52 us
  transfers between devices with their start and end apart: 4, of which 3 were waited for; matrix products, arithmetic and copies ran while one was open for 8% of the time, Pallas kernels for 0%

commit v1 on v0

--- a/solution.py
+++ b/solution.py
@@ -10,6 +10,16 @@
 alpha_act = 1.702
 limit_act = 7.0
 negative = -1e30
+
+
+def around_the_ring(block, axis, dim):
+    count = lax.axis_size(axis)
+    held, blocks = (block, [block])
+    for _ in range(count - 1):
+        held = lax.ppermute(held, axis, [(i, (i + 1) % count) for i in range(count)])
+        blocks.insert(0, held)
+    flat = jnp.concatenate(blocks, axis=dim)
+    return jnp.roll(flat, (lax.axis_index(axis) + 1) * block.shape[dim], axis=dim)
 
 
 def clamped_unit(gate, up):
@@ -63,7 +73,7 @@
     initial = (lowest, nothing, blank, lowest, nothing, blank)
     piece_a = lax.all_gather(keys_a, "ep", axis=0, tiled=True)
     piece_b = lax.all_gather(keys_b, "ep", axis=0, tiled=True)
-    piece_v = lax.all_gather(values, "ep", axis=0, tiled=True)
+    piece_v = around_the_ring(values, "ep", 0)
     count = piece_a.shape[0]
 
     def visit(state):

time: 351 us -> 279 us (0.79)
  blocking collectives: 158 us -> 97.8 us
  waiting for transfers between devices: 110 us -> 87.4 us
  local copies, waits for them, and re-layouts: 16.1 us -> 27.5 us
    reduce_scatter x1, waiting for transfers between devices: 58.9 us -> 0.01 us  [experts(): lax.psum_scatter(jnp.dot(hidden, w_down[0], preferred_element_type=jnp.fl...]
    ppermute x0 -> x7, waiting for transfers between devices: none -> 32 us  [around_the_ring(): lax.ppermute(held, axis, [(i, (i + 1) % count) for i in range(count)])]
    all_gather x1 -> x0, blocking collectives: 31.3 us -> none  [mixer(): piece_v = lax.all_gather(values, 'ep', axis=0, tiled=True)]
    all_gather x1, blocking collectives: 54.2 us -> 27.1 us  [mixer(): piece_a = lax.all_gather(keys_a, 'ep', axis=0, tiled=True)]
    unnamed x22 -> x40, local copies, waits for them, and re-layouts: 1.32 us -> 11.9 us
    ppermute x0 -> x7, starting transfers between devices: none -> 3.54 us  [around_the_ring(): lax.ppermute(held, axis, [(i, (i + 1) % count) for i in range(count)])]
  transfers between devices with their start and end apart: 4 -> 11, of which waited for: 3 -> 8; matrix products, arithmetic and copies ran while one was open for 8% -> 13% of each run, Pallas kernels for 0% -> 0%
where the time goes in v1:
time: 279 us; the launch traced here: 278 us
  blocking collectives  97.8 us (35%)
  waiting for transfers between devices  87.4 us (31%)
  matrix products  29.2 us (10%)
  local copies, waits for them, and re-layouts  27.5 us (10%)
  between operations  14.6 us (5%)
  other arithmetic  13.3 us (5%)
  starting transfers between devices  8.1 us (3%)
    all_gather x1, waiting for transfers between devices, experts(): lax.all_gather(arrived, 'tp', axis=0, tiled=True)  45.5 us
    all_to_all x1, blocking collectives, experts(): lax.all_to_all(outgoing, 'ep', split_axis=0, concat_axis=1, tiled=True)  44.2 us
    ppermute x7, waiting for transfers between devices, around_the_ring(): lax.ppermute(held, axis, [(i, (i + 1) % count) for i in range(count)])  32 us
    all_gather x1, blocking collectives, mixer(): piece_a = lax.all_gather(keys_a, 'ep', axis=0, tiled=True)  27.1 us
    all_gather x1, blocking collectives, mixer(): piece_b = lax.all_gather(keys_b, 'ep', axis=0, tiled=True)  26.5 us
    dot_general x1, matrix products, experts(): jnp.dot(hidden, w_down[0], preferred_element_type=jnp.float32)  11.9 us
    unnamed x40, local copies, waits for them, and re-layouts  11.9 us
    reduce_scatter x1, waiting for transfers between devices, mixer(): lax.psum_scatter(jnp.einsum('gjrv,gjvd->rd', heads_out, weights_out, pref...  8.68 us
  transfers between devices with their start and end apart: 11, of which 8 were waited for; matrix products, arithmetic and copies ran while one was open for 13% of the time, Pallas kernels for 0%

profile of v1, /device:TPU:0, one launch (start us, length us, event | category | flops | bytes accessed | tf_op | source)
XLA Modules:
  0.0 278.0 jit_solution(17752843123987090205)
XLA Ops:
  7.2 0.9 copy.55
  8.4 0.7 broadcast_multiply_fusion
  10.3 1.4 scatter_custom_fusion
  12.0 1.2 fusion.25
  13.2 1.2 fusion.27
  14.4 3.1 %gather_fusion = bf16[384,2048]{1,0:T(8,128)(2,1)} fusion(bf16[128,2048]{1,0:T(8,128)(2,1)S(1)} %fusion.27, s32[1024]{0:T(1024)S(1)} %pad_clamp_fusion.1), kind=kCustom, calls=%fused_computation | custom fusion | bytes 3147264 | tf_op jit(solution)/shard_map/jit(_take)/gather | solution.py:39
  17.6 1.7 select_select_fusion
  19.2 44.2 %all_to_all.14 = bf16[8,48,2048]{2,1,0:T(8,128)(2,1)} all-to-all(bf16[8,48,2048]{2,1,0:T(8,128)(2,1)S(1)} %select_select_fusion), channel_id=1, replica_groups=mesh['ep'=8,'tp'=4] {'ep'}, dimensions={0} | all-to-all | bytes 3145728 | tf_op jit(solution)/shard_map/all_to_all | solution.py:127
  63.5 45.5 %all-gather.2.cloned.1.call-done = bf16[1536,2048]{1,0:T(8,128)(2,1)} async-done(((bf16[384,2048]{1,0:T(8,128)(2,1)}), bf16[1536,2048]{1,0:T(8,128)(2,1)}) %all-gather.2.cloned.1.call-update) | async-done | bytes 6291472 | tf_op jit(solution)/shard_map/all_gather | solution.py:130
  109.0 8.5 %convolution_minimum_fusion = f32[1536,512]{1,0:T(8,128)} fusion(bf16[1536,2048]{1,0:T(8,128)(2,1)} %all-gather.2.cloned.1.call-done, bf16[1,2048,512]{2,1,0:T(8,128)(2,1)} %param.29), kind=kOutput, calls=%fused_computation.29 | convolution fusion | flops 3222011904 | bytes 11534336 | tf_op jit(solution)/shard_map/dot_general | solution.py:32
  117.5 11.9 %convolution_convert_fusion = bf16[1536,2048]{1,0:T(8,128)(2,1)} fusion(bf16[1,512,2048]{2,1,0:T(8,128)(2,1)S(1)} %copy-done, bf16[1536,2048]{1,0:T(8,128)(2,1)} %all-gather.2.cloned.1.call-done, f32[1536,512]{1,0:T(8,128)} %convolution_minimum_fusion, bf16[1,2048,512]{2,1,0:T(8,128)(2,1)} %param.30), kind=kOutput, calls=%fused_computation.27 | convolution fusion | flops 6452674560 | bytes 19922944 | tf_op jit(solution)/shard_map/dot_general | solution.py:132
  129.5 0.8 copy-done.3
  130.4 1.5 collective-permute-start
  131.9 5.5 %collective-permute-done = bf16[128,256]{0,1:T(8,128)(2,1)S(1)} collective-permute-done((bf16[128,256]{0,1:T(8,128)(2,1)S(1)}, bf16[128,256]{0,1:T(8,128)(2,1)S(1)}, u32[]{:S(2)}, u32[]{:S(2)}) %collective-permute-start) | collective-permute-done | bytes 65568 | tf_op jit(solution)/shard_map/ppermute | solution.py:19
  137.4 7.0 %collective-permute-done.1 = bf16[128,256]{0,1:T(8,128)(2,1)S(1)} collective-permute-done((bf16[128,256]{0,1:T(8,128)(2,1)S(1)}, bf16[128,256]{0,1:T(8,128)(2,1)S(1)}, u32[]{:S(2)}, u32[]{:S(2)}) %collective-permute-start.1) | collective-permute-done | bytes 65568 | tf_op jit(solution)/shard_map/ppermute | solution.py:19
  144.4 7.0 %collective-permute-done.2 = bf16[128,256]{0,1:T(8,128)(2,1)S(1)} collective-permute-done((bf16[128,256]{0,1:T(8,128)(2,1)S(1)}, bf16[128,256]{0,1:T(8,128)(2,1)S(1)}, u32[]{:S(2)}, u32[]{:S(2)}) %collective-permute-start.2) | collective-permute-done | bytes 65568 | tf_op jit(solution)/shard_map/ppermute | solution.py:19
  151.6 6.7 %collective-permute-done.3 = bf16[128,256]{0,1:T(8,128)(2,1)S(1)} collective-permute-done((bf16[128,256]{0,1:T(8,128)(2,1)S(1)}, bf16[128,256]{0,1:T(8,128)(2,1)S(1)}, u32[]{:S(2)}, u32[]{:S(2)}) %collective-permute-start.3) | collective-permute-done | bytes 65568 | tf_op jit(solution)/shard_map/ppermute | solution.py:19
  159.7 5.8 %collective-permute-done.4 = bf16[128,256]{0,1:T(8,128)(2,1)S(1)} collective-permute-done((bf16[128,256]{0,1:T(8,128)(2,1)S(1)}, bf16[128,256]{0,1:T(8,128)(2,1)S(1)}, u32[]{:S(2)}, u32[]{:S(2)}) %collective-permute-start.4) | collective-permute-done | bytes 65568 | tf_op jit(solution)/shard_map/ppermute | solution.py:19
  165.5 26.5 %all_gather.10 = bf16[1024,128]{0,1:T(8,128)(2,1)S(1)} all-gather(bf16[128,128]{0,1:T(8,128)(2,1)S(1)} %copy.52), channel_id=1, replica_groups=mesh['ep'=8,'tp'=4] {'ep'}, dimensions={0}, use_global_device_ids=true | all-gather | bytes 294912 | tf_op jit(solution)/shard_map/all_gather | solution.py:75
  192.0 2.0 collective-permute-start.6
  194.0 27.1 %all_gather.9 = bf16[1024,128]{0,1:T(8,128)(2,1)S(1)} all-gather(bf16[128,128]{0,1:T(8,128)(2,1)S(1)} %copy.48), channel_id=1, replica_groups=mesh['ep'=8,'tp'=4] {'ep'}, dimensions={0}, use_global_device_ids=true | all-gather | bytes 294912 | tf_op jit(solution)/shard_map/all_gather | solution.py:74
  221.0 0.7 constant_dynamic-update-slice_fusion.15
  221.7 0.7 constant_dynamic-update-slice_fusion.14
  222.3 0.6 constant_dynamic-update-slice_fusion.13
  223.0 0.6 constant_dynamic-update-slice_fusion.12
  223.6 4.4 %all-to-all-start.1 = ((bf16[8,48,2048]{2,1,0:T(8,128)(2,1)}), bf16[8,48,2048]{2,1,0:T(8,128)(2,1)}, u32[]{:S(2)}, u32[]{:S(2)}) async-start(bf16[8,48,2048]{2,1,0:T(8,128)(2,1)} %bitcast.83), calls=%async_computation.3 | async-start | bytes 3145728 | tf_op jit(solution)/shard_map/all_to_all | solution.py:137
  228.8 0.7 constant_dynamic-update-slice_fusion.10
  230.1 0.7 constant_dynamic-update-slice_fusion.8
  230.7 0.7 constant_dynamic-update-slice_fusion.7
  231.4 0.6 constant_dynamic-update-slice_fusion.6
  232.0 0.6 constant_dynamic-update-slice_fusion.5
  233.3 0.6 constant_dynamic-update-slice_fusion.3
  233.9 0.6 constant_dynamic-update-slice_fusion.2
  235.2 0.7 constant_dynamic-update-slice_fusion
  235.9 10.1 %conditional.1 = (f32[2,2,128]{2,1,0:T(2,128)S(1)}, f32[2,2,128,128]{3,2,1,0:T(8,128)S(1)}, f32[2,2,128]{2,1,0:T(2,128)S(1)}, f32[2,2,128,128]{3,2,1,0:T(8,128)S(1)}) conditional(s32[]{:T(128)} %bitcast, () %tuple.27, (s32[128]{0:T(128)S(1)}, bf16[1024,128]{0,1:T(8,128)(2,1)S(1)}, bf16[128,256]{1,0:T(8,128)(2,1)S(1)}, s32[]{:T(128)}, s32[]{:T(128)}, ...), branch_computations={%region_0.1_spmd, %region_1.6_spmd.clone} | conditional | flops 416414720 | bytes 29385456 | solution.py:91
  235.9 2.1 constant_dynamic-slice_fusion
  238.2 1.8 fusion.40
  240.2 2.3 fusion.1
  242.5 0.9 fusion.6
  243.4 0.7 copy-done.1
  244.1 0.8 fusion.8
  245.0 1.0 fusion.5
  246.4 2.9 %fusion.21 = bf16[128,2048]{1,0:T(8,128)(2,1)} fusion(bf16[2,2,128,2048]{3,2,1,0:T(8,128)(2,1)} %bitcast.82, f32[2,2,128,128]{3,2,1,0:T(8,128)S(1)} %get-tuple-element.196, f32[128]{0:T(128)S(1)} %copy-done.10, f32[2,2,128]{2,1,0:T(2,128)S(1)} %add_rsqrt_fusion), kind=kOutput, calls=%fused_computation.34 | convolution fusion | flops 268894208 | bytes 2886144 | tf_op jit(solution)/shard_map/gjrv,gjvd->rd/dot_general | solution.py:100
  249.8 1.2 all-to-all-done.1
  251.0 4.0 %gather_fusion.1 = bf16[256,2048]{1,0:T(8,128)(2,1)S(1)} fusion(bf16[384,2048]{1,0:T(8,128)(2,1)} %bitcast.14, s32[1024]{0:T(1024)S(1)} %pad_clamp_fusion), kind=kCustom, calls=%fused_computation.1 | custom fusion | bytes 2098176 | tf_op jit(solution)/shard_map/jit(_take)/gather | solution.py:140
  255.0 1.5 gather.15
  256.5 6.3 %multiply_reduce_fusion = bf16[128,2048]{1,0:T(8,128)(2,1)} fusion(bf16[128,2,2048]{2,1,0:T(2,128)(2,1)} %gather.15, pred[128,2]{1,0:T(8,128)(4,1)S(1)} %copy.58, f32[128,2]{1,0:T(8,128)S(1)} %copy.60), kind=kLoop, calls=%fused_computation.38 | loop fusion | flops 1835008 | bytes 1574144 | tf_op jit(solution)/shard_map/reduce_sum | solution.py:141
  262.8 8.7 %reduce-scatter.3.cloned.1.call-done = bf16[32,2048]{1,0:T(8,128)(2,1)} async-done(((bf16[128,2048]{1,0:T(8,128)(2,1)}), bf16[32,2048]{1,0:T(8,128)(2,1)}) %reduce-scatter.3.cloned.1.call-update) | async-done | bytes 131088 | tf_op jit(solution)/shard_map/reduce_scatter | solution.py:99
  (77 shorter events, 6.6 us)
Async XLA Ops:
  7.2 110.4 %copy-start = (bf16[1,512,2048]{2,1,0:T(8,128)(2,1)S(1)}, bf16[1,512,2048]{2,1,0:T(8,128)(2,1)}, u32[]{:S(2)}) copy-start(bf16[1,512,2048]{2,1,0:T(8,128)(2,1)} %param.31) | copy-start | bytes 6291460
  7.2 101.8 %all-gather.2.cloned.1.call-start = ((), (), s32[]{:S(2)}) async-start(), calls=%async_computation.5 | async-start | bytes 7864320 | tf_op jit(solution)/shard_map/all_gather | solution.py:130
  63.5 160.2 %reduce-scatter.5.cloned.1.call-start = ((), (), s32[]{:S(2)}) async-start(), calls=%async_computation.6 | async-start | bytes 7864320 | tf_op jit(solution)/shard_map/reduce_scatter | solution.py:131
  129.5 0.8 copy-start.3
  129.5 21.9 %copy-start.6 = (bf16[128,128]{1,0:T(8,128)(2,1)S(1)}, bf16[128,128]{1,0:T(8,128)(2,1)}, u32[]{:S(2)}) copy-start(bf16[128,128]{1,0:T(8,128)(2,1)} %param.20) | copy-start | bytes 98308
  129.5 22.0 %copy-start.7 = (bf16[128,128]{1,0:T(8,128)(2,1)S(1)}, bf16[128,128]{1,0:T(8,128)(2,1)}, u32[]{:S(2)}) copy-start(bf16[128,128]{1,0:T(8,128)(2,1)} %param.19) | copy-start | bytes 98308
  129.5 30.1 %copy-start.11 = (f32[4]{0:T(128)S(1)}, f32[4]{0:T(128)}, u32[]{:S(2)}) copy-start(f32[4]{0:T(128)} %param.22) | copy-start | bytes 52
  130.4 7.0 %collective-permute-start = (bf16[128,256]{0,1:T(8,128)(2,1)S(1)}, bf16[128,256]{0,1:T(8,128)(2,1)S(1)}, u32[]{:S(2)}, u32[]{:S(2)}) collective-permute-start(bf16[128,256]{0,1:T(8,128)(2,1)S(1)} %copy.49), channel_id=1, source_target_pairs={{0,4},{4,8},{8,12},{12,16},{16,20},{20,24},{24,28},{28,0},{1,5},{5... | collective-permute-start | bytes 196616 | tf_op jit(solution)/shard_map/ppermute | solution.py:19
  137.4 7.0 %collective-permute-start.1 = (bf16[128,256]{0,1:T(8,128)(2,1)S(1)}, bf16[128,256]{0,1:T(8,128)(2,1)S(1)}, u32[]{:S(2)}, u32[]{:S(2)}) collective-permute-start(bf16[128,256]{0,1:T(8,128)(2,1)S(1)} %collective-permute-done), channel_id=1, source_target_pairs={{0,4},{4,8},{8,12},{12,16},{16,20},{20,24},{24,28},{28,0},{1,5},{5... | collective-permute-start | bytes 196616 | tf_op jit(solution)/shard_map/ppermute | solution.py:19
  144.4 7.0 %collective-permute-start.2 = (bf16[128,256]{0,1:T(8,128)(2,1)S(1)}, bf16[128,256]{0,1:T(8,128)(2,1)S(1)}, u32[]{:S(2)}, u32[]{:S(2)}) collective-permute-start(bf16[128,256]{0,1:T(8,128)(2,1)S(1)} %collective-permute-done.1), channel_id=1, source_target_pairs={{0,4},{4,8},{8,12},{12,16},{16,20},{20,24},{24,28},{28,0},{1,5},{5... | collective-permute-start | bytes 196616 | tf_op jit(solution)/shard_map/ppermute | solution.py:19
  151.4 7.0 %collective-permute-start.3 = (bf16[128,256]{0,1:T(8,128)(2,1)S(1)}, bf16[128,256]{0,1:T(8,128)(2,1)S(1)}, u32[]{:S(2)}, u32[]{:S(2)}) collective-permute-start(bf16[128,256]{0,1:T(8,128)(2,1)S(1)} %collective-permute-done.2), channel_id=1, source_target_pairs={{0,4},{4,8},{8,12},{12,16},{16,20},{20,24},{24,28},{28,0},{1,5},{5... | collective-permute-start | bytes 196616 | tf_op jit(solution)/shard_map/ppermute | solution.py:19
  158.3 7.2 %collective-permute-start.4 = (bf16[128,256]{0,1:T(8,128)(2,1)S(1)}, bf16[128,256]{0,1:T(8,128)(2,1)S(1)}, u32[]{:S(2)}, u32[]{:S(2)}) collective-permute-start(bf16[128,256]{0,1:T(8,128)(2,1)S(1)} %collective-permute-done.3), channel_id=1, source_target_pairs={{0,4},{4,8},{8,12},{12,16},{16,20},{20,24},{24,28},{28,0},{1,5},{5... | collective-permute-start | bytes 196616 | tf_op jit(solution)/shard_map/ppermute | solution.py:19
  165.5 26.5 %collective-permute-start.5 = (bf16[128,256]{0,1:T(8,128)(2,1)S(1)}, bf16[128,256]{0,1:T(8,128)(2,1)S(1)}, u32[]{:S(2)}, u32[]{:S(2)}) collective-permute-start(bf16[128,256]{0,1:T(8,128)(2,1)S(1)} %collective-permute-done.4), channel_id=1, source_target_pairs={{0,4},{4,8},{8,12},{12,16},{16,20},{20,24},{24,28},{28,0},{1,5},{5... | collective-permute-start | bytes 196616 | tf_op jit(solution)/shard_map/ppermute | solution.py:19
  192.0 29.1 %collective-permute-start.6 = (bf16[128,256]{0,1:T(8,128)(2,1)S(1)}, bf16[128,256]{0,1:T(8,128)(2,1)S(1)}, u32[]{:S(2)}, u32[]{:S(2)}) collective-permute-start(bf16[128,256]{0,1:T(8,128)(2,1)S(1)} %collective-permute-done.5), channel_id=1, source_target_pairs={{0,4},{4,8},{8,12},{12,16},{16,20},{20,24},{24,28},{28,0},{1,5},{5... | collective-permute-start | bytes 196616 | tf_op jit(solution)/shard_map/ppermute | solution.py:19
  223.6 12.2 %copy-start.4 = (bf16[128,256]{1,0:T(8,128)(2,1)S(1)}, bf16[128,256]{1,0:T(8,128)(2,1)}, u32[]{:S(2)}) copy-start(bf16[128,256]{1,0:T(8,128)(2,1)} %param.17) | copy-start | bytes 196612
  223.6 12.2 %copy-start.5 = (bf16[128,256]{1,0:T(8,128)(2,1)S(1)}, bf16[128,256]{1,0:T(8,128)(2,1)}, u32[]{:S(2)}) copy-start(bf16[128,256]{1,0:T(8,128)(2,1)} %param.18) | copy-start | bytes 196612
  223.6 27.4 %all-to-all-start.1 = ((bf16[8,48,2048]{2,1,0:T(8,128)(2,1)}), bf16[8,48,2048]{2,1,0:T(8,128)(2,1)}, u32[]{:S(2)}, u32[]{:S(2)}) async-start(bf16[8,48,2048]{2,1,0:T(8,128)(2,1)} %bitcast.83), calls=%async_computation.3 | async-start | bytes 3145728 | tf_op jit(solution)/shard_map/all_to_all | solution.py:137
  228.1 43.4 %reduce-scatter.3.cloned.1.call-start = ((), (), s32[]{:S(2)}) async-start(), calls=%async_computation.4 | async-start | bytes 655360 | tf_op jit(solution)/shard_map/reduce_scatter | solution.py:99
  235.9 10.5 %copy-start.10 = (f32[128]{0:T(128)S(1)}, f32[128]{0:T(128)}, u32[]{:S(2)}) copy-start(f32[128]{0:T(128)} %param.23) | copy-start | bytes 1540
  240.2 2.3 copy-start.2
  242.5 1.6 copy-start.1
  246.0 3.5 %copy-start.8 = (s32[128,2]{0,1:T(2,128)S(1)}, s32[128,2]{0,1:T(2,128)}, u32[]{:S(2)}) copy-start(s32[128,2]{0,1:T(2,128)} %param.27) | copy-start | bytes 3076
  246.0 3.7 %copy-start.9 = (f32[128,2]{0,1:T(2,128)S(1)}, f32[128,2]{0,1:T(2,128)}, u32[]{:S(2)}) copy-start(f32[128,2]{0,1:T(2,128)} %param.28) | copy-start | bytes 3076
Sparse Core Ops, SparseCore 0:
  63.6 45.3 all-gather.1
  129.6 58.8 reduce-scatter.4
  249.4 22.0 reduce-scatter.2
